TPU v7x, 256 devices: a 2x2x32 block of a 4x8x32 slice. The times are simulated.
256 devices in a mesh: grp: 4 (over y, x), ep: 32 (over z), tp: 2 (over core).
Axes of the slice: x: 2, y: 2, z: 32, core: 2. Of those that a mesh axis runs over, the one named last changes fastest.
The devices are a block of a 4x8x32 slice.
Arguments:
- tokens: bfloat16 [16384, 4096], P(('grp', 'ep')), parts along dimension 0, may hold values from -16 to 16, as said below
- norm_gain: float32 [4096], replicated, may hold values from 0.1 to 1.9
- gate_weight: bfloat16 [32, 4096, 768], P('ep', None, 'tp'), may hold values from -0.09375 to 0.09375
- up_weight: bfloat16 [32, 4096, 768], P('ep', None, 'tp'), may hold values from -0.09375 to 0.09375
- down_weight: bfloat16 [32, 768, 4096], P('ep', 'tp'), may hold values from -0.21875 to 0.21875
- chosen: int32 [128, 32, 20], P(('grp', 'ep')), parts along dimension 0, may hold values from 0 to 128, as said below
- affinity: float32 [128, 32, 20], P(('grp', 'ep')), parts along dimension 0, may hold values from 0.2 to 1
Outputs:
- mixed: bfloat16 [16384, 4096], P(('grp', 'ep'), 'tp'), parts along dimension 0
There are 4 independent parts, one for each index of `grp`. A program takes and returns all parts, laid end to end along the dimension named above; an argument that names none is the same for every part. Nothing has to cross between parts.
Inputs may be any that keep to these rules, and one draw needn't show every extreme that they name: `tokens`: draws differ in their scale from row to row. `chosen`: in each (block, expert) row the live entries come first and are distinct; dead entries equal 128. Every expert has exactly 512 live slots in all and at least one live slot in every block; some block gives some expert exactly 20 live slots.
All inputs are finite; a program needn't handle non-finite values.
Results may differ from a plain program's by a relative error of at most 0.0095.
Values may be sent and summed in bfloat16 or wider, within the bound.
A program may use at most 64 MiB of HBM per device.

v0:
```python
import jax
import jax.numpy as jnp
from jax import lax
from jax.sharding import PartitionSpec as P

norm_eps = 1e-06


def cut_along(shard, dim, size):
    before, after = (shard.shape[:dim], shard.shape[dim + 1 :])
    return jnp.moveaxis(shard.reshape(*before, size, -1, *after), dim, 0)


def summed_on_arrival(shard, axis, dim):
    size = lax.axis_size(axis)
    pieces = lax.all_to_all(cut_along(shard, dim, size), axis, 0, 0, tiled=True)
    return jnp.sum(pieces.astype(jnp.float32), axis=0)


def normalize(block, norm_gain):
    values = block.astype(jnp.float32)
    scaled = values * lax.rsqrt(jnp.mean(values * values, axis=-1, keepdims=True) + norm_eps)
    return (scaled * norm_gain).astype(jnp.bfloat16)


def shards(tokens, norm_gain, gate_weight, up_weight, down_weight, chosen, affinity):
    tok_rows = tokens.shape[0]
    model_width = tokens.shape[1]
    slot_count = chosen.shape[2]
    picked_rows = chosen[0]
    source = normalize(tokens, norm_gain)
    half_slots = slot_count // 2
    own_slots = lax.dynamic_slice_in_dim(
        picked_rows, lax.axis_index("tp") * half_slots, half_slots, 1
    )
    outgoing = jnp.take(source, own_slots, axis=0, mode="clip")
    landed = lax.all_to_all(outgoing, "ep", split_axis=0, concat_axis=0, tiled=True)
    arrived = lax.all_gather(landed, "tp", axis=1, tiled=True)
    arrived_rows = arrived.reshape(-1, model_width)
    gate_proj = jnp.dot(arrived_rows, gate_weight[0], preferred_element_type=jnp.float32)
    up_value = jnp.dot(arrived_rows, up_weight[0], preferred_element_type=jnp.float32)
    hidden = (jax.nn.silu(gate_proj) * up_value).astype(jnp.bfloat16)
    columns = down_weight[0]
    summed = summed_on_arrival(
        lax.dot_general(
            columns, hidden, (((0,), (1,)), ((), ())), preferred_element_type=jnp.float32
        ).astype(jnp.bfloat16),
        "tp",
        0,
    )
    expert_out = summed.astype(jnp.bfloat16)
    returned = lax.all_to_all(expert_out, "ep", split_axis=1, concat_axis=1, tiled=True)
    weight = jnp.where(picked_rows < tok_rows, affinity[0], 0.0).astype(jnp.bfloat16).reshape(-1)
    flat_picks = picked_rows.reshape(-1)
    matches = flat_picks[None, :] == jnp.arange(tok_rows, dtype=jnp.int32)[:, None]
    combine = jnp.where(matches, weight[None, :], jnp.zeros((), jnp.bfloat16))
    mixed = lax.dot_general(
        combine, returned, (((1,), (1,)), ((), ())), preferred_element_type=jnp.float32
    )
    return mixed.astype(jnp.bfloat16)


def solution(mesh):
    in_specs = (
        P(("grp", "ep"), None),
        P(),
        P("ep", None, "tp"),
        P("ep", None, "tp"),
        P("ep", "tp", None),
        P(("grp", "ep"), None, None),
        P(("grp", "ep"), None, None),
    )
    out_specs = P(("grp", "ep"), "tp")
    return jax.shard_map(shards, mesh=mesh, in_specs=in_specs, out_specs=out_specs, check_vma=False)
```

profile of v0, /device:TPU:37, one launch (start us, length us, event | category | flops | bytes accessed | tf_op | source)
XLA Modules:
  0.0 827.9 jit_solution(3953942204151701795)
XLA Ops:
  6.5 0.0 copy-start
  6.6 0.0 all-gather.2.cloned.1.call-start
  6.6 0.8 constant_dynamic-slice_fusion
  7.4 0.1 copy.13
  7.5 0.1 reshape.35
  7.6 1.5 fusion.5
  9.1 2.5 fusion.7
  11.7 9.4 %gather_fusion = bf16[320,4096]{1,0:T(8,128)(2,1)} fusion(bf16[128,4096]{1,0:T(8,128)(2,1)} %fusion.7, s32[1024]{0:T(1024)S(1)} %pad_clamp_fusion), kind=kCustom, calls=%fused_computation | custom fusion | bytes 5244160 | tf_op jit(solution)/shard_map/jit(_take)/gather | solution.py:36
  21.1 4.6 reshape.34
  25.7 407.3 %all_to_all.22 = bf16[32,10,4096]{2,1,0:T(8,128)(2,1)S(1)} all-to-all(bf16[32,10,4096]{2,1,0:T(8,128)(2,1)} %reshape.34), channel_id=1, replica_groups=mesh['grp'=4,'ep'=32,'tp'=2] {'ep'}, dimensions={0} | all-to-all | bytes 5242880 | tf_op jit(solution)/shard_map/all_to_all | solution.py:37
  433.0 2.9 copy.14
  435.9 0.1 all-gather.2.cloned.1.call-update
  436.0 20.9 %all-gather.2.cloned.1.call-done = bf16[32,20,4096]{2,0,1:T(8,128)(2,1)} async-done(((bf16[32,10,4096]{2,0,1:T(8,128)(2,1)}), bf16[32,20,4096]{2,0,1:T(8,128)(2,1)}) %all-gather.2.cloned.1.call-update) | async-done | bytes 5242896 | tf_op jit(solution)/shard_map/all_gather | solution.py:38
  456.8 8.1 copy.15
  464.9 7.8 reshape.31
  472.7 7.3 fusion.3
  480.1 0.0 copy-done
  480.1 11.6 %convolution_convert_fusion = bf16[640,4096]{1,0:T(8,128)(2,1)} fusion(bf16[1,384,4096]{2,1,0:T(8,128)(2,1)S(1)} %copy-done, bf16[640,4096]{1,0:T(8,128)(2,1)} %reshape.31, bf16[1,4096,384]{2,1,0:T(8,128)(2,1)} %param.10, f32[640,384]{1,0:T(8,128)} %fusion.3), kind=kOutput, calls=%fused_computation.1 | convolution fusion | flops 4030627840 | bytes 17760256 | tf_op jit(solution)/shard_map/dot_general | solution.py:45
  491.7 2.9 copy.19
  494.6 9.1 %all_to_all.23 = bf16[2,2048,640]{1,2,0:T(8,128)(2,1)} all-to-all(bf16[2,2048,640]{1,2,0:T(8,128)(2,1)S(1)} %bitcast.27), channel_id=1, replica_groups=mesh['grp'=4,'ep'=32,'tp'=2] {'tp'}, dimensions={0} | all-to-all | bytes 10485760 | tf_op jit(solution)/shard_map/all_to_all | solution.py:16
  503.7 6.0 reduce_sum.22
  509.7 5.1 all_to_all.16
  514.8 0.0 copy-start.1
  514.8 0.0 copy-start.2
  514.8 21.9 %all-to-all-start.2 = ((bf16[2048,32,20]{0,2,1:T(8,128)(2,1)}), bf16[2048,32,20]{0,2,1:T(8,128)(2,1)}, u32[]{:S(2)}, u32[]{:S(2)}) async-start(bf16[2048,32,20]{0,2,1:T(8,128)(2,1)} %all_to_all.16), calls=%async_computation.2 | async-start | bytes 6291456 | tf_op jit(solution)/shard_map/all_to_all | solution.py:52
  536.8 0.0 copy-done.1
  536.8 0.1 copy.11
  536.8 0.1 eq.15
  536.9 0.0 copy-done.2
  537.0 0.1 copy.12
  537.0 0.1 squeeze.13
  537.2 275.6 %all-to-all-done.2 = bf16[2048,32,20]{0,2,1:T(8,128)(2,1)} async-done(((bf16[2048,32,20]{0,2,1:T(8,128)(2,1)}), bf16[2048,32,20]{0,2,1:T(8,128)(2,1)}, u32[]{:S(2)}, u32[]{:S(2)}) %all-to-all-start.2) | async-done | bytes 2621472 | tf_op jit(solution)/shard_map/all_to_all | solution.py:52
  812.7 5.2 all_to_all.18
  817.9 3.1 convolution_convert_fusion.1
  (3 shorter events, 0.0 us)
Async XLA Ops:
  6.5 473.5 %copy-start = (bf16[1,384,4096]{2,1,0:T(8,128)(2,1)S(1)}, bf16[1,384,4096]{2,1,0:T(8,128)(2,1)}, u32[]{:S(2)}) copy-start(bf16[1,384,4096]{2,1,0:T(8,128)(2,1)} %param.11) | copy-start | bytes 9437188
  6.6 450.3 %all-gather.2.cloned.1.call-start = ((), (), s32[]{:S(2)}) async-start(), calls=%async_computation.3 | async-start | bytes 7864320 | tf_op jit(solution)/shard_map/all_gather | solution.py:38
  514.8 21.9 %copy-start.1 = (s32[1,32,20]{1,0,2:T(1,128)S(1)}, s32[1,32,20]{1,0,2:T(1,128)}, u32[]{:S(2)}) copy-start(s32[1,32,20]{1,0,2:T(1,128)} %param.12) | copy-start | bytes 7684
  514.8 22.1 %copy-start.2 = (f32[1,32,20]{1,0,2:T(1,128)S(1)}, f32[1,32,20]{1,0,2:T(1,128)}, u32[]{:S(2)}) copy-start(f32[1,32,20]{1,0,2:T(1,128)} %param.13) | copy-start | bytes 7684
  514.8 297.9 %all-to-all-start.2 = ((bf16[2048,32,20]{0,2,1:T(8,128)(2,1)}), bf16[2048,32,20]{0,2,1:T(8,128)(2,1)}, u32[]{:S(2)}, u32[]{:S(2)}) async-start(bf16[2048,32,20]{0,2,1:T(8,128)(2,1)} %all_to_all.16), calls=%async_computation.2 | async-start | bytes 6291456 | tf_op jit(solution)/shard_map/all_to_all | solution.py:52
Sparse Core Ops, SparseCore 0:
  436.1 20.6 all-gather.1
where the time goes:
time: 833 us; the launch traced here: 828 us
  blocking collectives  416 us (50%)
  waiting for transfers between devices  296 us (36%)
  local copies, waits for them, and re-layouts  47.6 us (6%)
  matrix products  22 us (3%)
  starting transfers between devices  21.9 us (3%)
  between operations  13.5 us (2%)
  other arithmetic  10.1 us (1%)
    all_to_all x1, blocking collectives, shards(): lax.all_to_all(outgoing, 'ep', split_axis=0, concat_axis=0, tiled=True)  407 us
    all_to_all x1, waiting for transfers between devices, shards(): lax.all_to_all(expert_out, 'ep', split_axis=1, concat_axis=1, tiled=True)  276 us
    all_to_all x1, starting transfers between devices, shards(): lax.all_to_all(expert_out, 'ep', split_axis=1, concat_axis=1, tiled=True)  21.9 us
    all_gather x1, waiting for transfers between devices, shards(): arrived = lax.all_gather(landed, 'tp', axis=1, tiled=True)  20.9 us
  transfers between devices with their start and end apart: 2, of which 2 were waited for; matrix products, arithmetic and copies ran while one was open for 0% of the time, Pallas kernels for 0%

commit v1 on v0

v1 whole, which is shorter than its diff:
```python
import functools

import jax
import jax.numpy as jnp
from jax import lax
from jax.experimental import pallas as pl
from jax.experimental.pallas import tpu as pltpu
from jax.sharding import PartitionSpec as P

norm_eps = 1e-06
UNIT = 32
REACH = 11
CHUNKS = 4
f32, bf16 = jnp.float32, jnp.bfloat16


def up8(rows):
    return -(-rows // 8) * 8


def dot(a, b):
    return jnp.dot(a, b, preferred_element_type=f32)


def dot_rows(a, b):
    return lax.dot_general(a, b, (((0,), (0,)), ((), ())), preferred_element_type=f32)


def kernel(
    n, reach, slots, tokens, gain, meta, gate_hbm, up_hbm, down_hbm, out,
    own, ring, mring, w_own, w_oth, d_own, d_oth, pk_own, pk_oth, eo, ps, po, psf, pof,
    far_out, far_in, red, top,
    wsem, dsend, drecv, msend, mrecv, pxs, pxr, pas, par, fs, fr, gs, gr, rs, rr,
):
    me, core = lax.axis_index("ep"), lax.axis_index("tp")
    far = n // 2 - reach
    chunks, trows, width = own.shape
    half = chunks * width
    hid = w_own.shape[1] // 2
    full_rows = up8(slots)
    base = slots // 2 // 8 * 8
    end_rows = up8(max(slots // 2, slots - base))
    partner = {"tp": 1 - core}
    sign = (1, -1)

    def at(offset):
        return {"ep": lax.rem(me + offset + n, n)}

    def rcopy(src, dst, s, r, dev):
        return pltpu.make_async_remote_copy(
            src_ref=src, dst_ref=dst, send_sem=s, recv_sem=r, device_id=dev,
            device_id_type=pl.DeviceIdType.MESH,
        )

    def far_rows(j):
        return full_rows if j < far else end_rows

    def hop(d, g, ch):
        src = own.at[ch] if d is None else ring.at[g, d, ch]
        nxt = 0 if d is None else d + 1
        return rcopy(src, ring.at[g, nxt, ch], dsend.at[g, nxt, ch], drecv.at[g, nxt, ch], at(sign[g]))

    def landed(d, g, ch):
        return rcopy(own.at[ch], ring.at[g, d, ch], dsend.at[g, d, ch], drecv.at[g, d, ch], at(sign[g]))

    def mhop(d, g):
        src = meta if d is None else mring.at[g, d]
        nxt = 0 if d is None else d + 1
        return rcopy(src, mring.at[g, nxt], msend.at[g, nxt], mrecv.at[g, nxt], at(sign[g]))

    def mlanded(d, g):
        return rcopy(meta, mring.at[g, d], msend.at[g, d], mrecv.at[g, d], at(sign[g]))

    def share(d):
        return rcopy(pk_own.at[d], pk_oth.at[d], pxs.at[d], pxr.at[d], partner)

    def give(src, d):
        return rcopy(src, eo.at[d], pas.at[d], par.at[d], partner)

    def far_send(g, j):
        rows = far_rows(j)
        return rcopy(
            far_out.at[g, j - 1, pl.ds(0, rows)], pk_own.at[reach + j, pl.ds(g * UNIT, rows)],
            fs.at[g, j - 1], fr.at[g, j - 1], at(sign[g] * j),
        )

    def far_back(g, j):
        rows = far_rows(j)
        return rcopy(
            eo.at[reach + j, pl.ds(g * UNIT, rows)], far_in.at[g, j - 1, pl.ds(0, rows)],
            gs.at[g, j - 1], gr.at[g, j - 1], at(-sign[g] * j),
        )

    def back(src, d, g, ch):
        return rcopy(src, red.at[g, d, ch], rs.at[g, d, ch], rr.at[g, d, ch], at(-sign[g]))

    lane = lax.broadcasted_iota(jnp.int32, (UNIT, meta.shape[1]), 1)
    tok = lax.broadcasted_iota(jnp.int32, (UNIT, trows), 1).astype(f32)
    slot = lax.broadcasted_iota(jnp.int32, (UNIT, 1), 0)

    def column(m, index):
        return jnp.sum(jnp.where(lane == index, m, 0.0), axis=1, keepdims=True)

    def hot(m, e, weighted, end=None):
        rows = column(m, e)
        value = column(m, n + e) if weighted else jnp.ones((UNIT, 1), f32)
        if end is not None:
            keep = (slot < slots // 2) if end == 0 else (slot >= slots // 2)
            rows = jnp.where(keep, rows, float(trows))
            if end == 1 and base:
                fill = jnp.full((base, 1), float(trows), f32)
                rows = jnp.concatenate([rows[base:], fill], axis=0)
                value = jnp.concatenate([value[base:], fill], axis=0)
        return jnp.where(rows == tok, value, 0.0)

    def far_hot(m, g, weighted):
        parts = []
        for j in range(1, far + 1):
            e = lax.rem(me + sign[g] * j + n, n)
            parts.append(hot(m, e, weighted, g if j == far else None))
        return jnp.concatenate(parts, axis=0).astype(bf16)

    loads = []
    for i, (src, dst) in enumerate((
        (gate_hbm.at[0, pl.ds(core * half, half)], w_own.at[:, pl.ds(0, hid)]),
        (up_hbm.at[0, pl.ds(core * half, half)], w_own.at[:, pl.ds(hid, hid)]),
        (gate_hbm.at[0, pl.ds((1 - core) * half, half)], w_oth.at[:, pl.ds(0, hid)]),
        (up_hbm.at[0, pl.ds((1 - core) * half, half)], w_oth.at[:, pl.ds(hid, hid)]),
        (down_hbm.at[0, :, pl.ds(pl.multiple_of(core * half, 128), half)], d_own),
        (down_hbm.at[0, :, pl.ds(pl.multiple_of((1 - core) * half, 128), half)], d_oth),
    )):
        loads.append(pltpu.make_async_copy(src, dst, wsem.at[i]))
        loads[-1].start()

    pk_own[0] = jnp.zeros_like(pk_own[0])
    for j in range(1, far + 1):
        pk_own[reach + j] = jnp.zeros_like(pk_own[reach + j])
        for g in range(2):
            far_in[g, j - 1] = jnp.zeros_like(far_in[g, j - 1])

    barrier = pltpu.get_barrier_semaphore()
    peers = [at(s * j) for j in range(1, far + 1) for s in sign] + [partner]
    for peer in peers:
        pl.semaphore_signal(barrier, inc=1, device_id=peer, device_id_type=pl.DeviceIdType.MESH)
    squares = jnp.zeros((trows, 1), f32)
    for i in range(2 * chunks):
        v = tokens[:, pl.ds(i * width, width)].astype(f32)
        squares += jnp.sum(v * v, axis=1, keepdims=True)
    scale = lax.rsqrt(squares / tokens.shape[1] + norm_eps)
    pl.semaphore_wait(barrier, len(peers))

    for g in range(2):
        mhop(None, g).start()
    for ch in range(chunks):
        cols = pl.ds(pl.multiple_of(core * half + ch * width, 128), width)
        own[ch] = (tokens[:, cols].astype(f32) * scale * gain[:, cols]).astype(bf16)
        for g in range(2):
            hop(None, g, ch).start()

    own_hot = hot(meta[...].astype(f32), me, False).astype(bf16)
    for ch in range(chunks):
        pk_own[0, pl.ds(0, UNIT), pl.ds(ch * width, width)] = dot(own_hot, own[ch]).astype(bf16)
    share(0).start()
    for load in loads:
        load.wait()

    def hidden_of(a, b):
        acc = dot(a, w_own[...]) + dot(b, w_oth[...])
        gate, upper = acc[:, :hid], acc[:, hid:]
        return (gate * jax.nn.sigmoid(gate) * upper).astype(bf16)

    def pick(t):
        for g in range(2):
            h = hot(mring[g, t - 1].astype(f32), me, False).astype(bf16)
            for ch in range(chunks):
                pk_own[t, pl.ds(g * UNIT, UNIT), pl.ds(ch * width, width)] = dot(h, ring[g, t - 1, ch]).astype(bf16)
        share(t).start()

    def pick_far():
        for g in range(2):
            h = far_hot(mring[g, reach - 1].astype(f32), g, False)
            for ch in range(chunks):
                y = dot(h, ring[g, reach - 1, ch]).astype(bf16)
                far_out[g, :, :, pl.ds(ch * width, width)] = y.reshape(far, UNIT, width)
        for j in range(far, 0, -1):
            for g in range(2):
                far_send(g, j).start()

    def expert(b):
        share(b).wait_recv()
        h = hidden_of(pk_own[b], pk_oth[b])
        spot = lax.rem(b, 2)

        @pl.when(b >= 2)
        def _():
            give(ps.at[spot], b - 2).wait_send()

        ps[spot] = dot(h, d_oth[...]).astype(bf16)
        give(ps.at[spot], b).start()
        po[spot] = dot(h, d_own[...]).astype(bf16)

    def finish(b):
        give(ps.at[0], b).wait_recv()
        eo[b] = (po[lax.rem(b, 2)].astype(f32) + eo[b].astype(f32)).astype(bf16)

    def step(t, carry):
        @pl.when(t <= reach)
        def _():
            for g in range(2):
                mlanded(t - 1, g).wait_recv()

                @pl.when(t < reach)
                def _():
                    mhop(t - 1, g).start()

        for ch in range(chunks):
            @pl.when(t <= reach)
            def _():
                for g in range(2):
                    landed(t - 1, g, ch).wait_recv()

                    @pl.when(t < reach)
                    def _():
                        hop(t - 1, g, ch).start()

            if ch == 0:
                @pl.when(t <= reach + 1)
                def _():
                    expert(t - 1)

            if ch == chunks - 2:
                @pl.when(t >= 2)
                def _():
                    finish(t - 2)

        @pl.when(t == reach)
        def _():
            pick_far()

        @pl.when(t <= reach)
        def _():
            pick(t)

        return carry

    lax.fori_loop(1, reach + 3, step, 0)

    for j in range(1, far + 1):
        for g in range(2):
            far_send(g, j).wait_recv()
        share(reach + j).start()
    for j in range(1, far + 1):
        share(reach + j).wait_recv()
    group = pl.ds(reach + 1, far)
    h = hidden_of(
        pk_own[group].reshape(far * 2 * UNIT, half), pk_oth[group].reshape(far * 2 * UNIT, half)
    )
    psf[...] = dot(h, d_oth[...]).astype(bf16).reshape(psf.shape)
    for j in range(far, 0, -1):
        give(psf.at[j - 1], reach + j).start()
    pof[...] = dot(h, d_own[...]).astype(bf16).reshape(pof.shape)
    for j in range(far, 0, -1):
        give(psf.at[j - 1], reach + j).wait_recv()
        eo[reach + j] = (pof[j - 1].astype(f32) + eo[reach + j].astype(f32)).astype(bf16)
        for g in range(2):
            far_back(g, j).start()

    own_w = hot(meta[...].astype(f32), me, True).astype(bf16)
    near_w = [hot(mring[g, reach - 1].astype(f32), me, True).astype(bf16) for g in range(2)]
    for j in range(far, 0, -1):
        for g in range(2):
            far_back(g, j).wait_recv()
    for g in range(2):
        fw = far_hot(mring[g, reach - 1].astype(f32), g, True)
        for ch in range(chunks):
            cols = pl.ds(ch * width, width)
            total = dot_rows(fw, far_in[g, :, :, cols].reshape(far * UNIT, width))
            total += dot_rows(near_w[g], eo[reach, pl.ds(g * UNIT, UNIT), cols])
            top[g, ch] = total.astype(bf16)
            back(top.at[g, ch], reach - 1, g, ch).start()

    def fold(i, carry):
        d = reach - i
        hots = [hot(mring[g, d - 1].astype(f32), me, True).astype(bf16) for g in range(2)]
        for ch in range(chunks):
            cols = pl.ds(ch * width, width)
            for g in range(2):
                add = dot_rows(hots[g], eo[d, pl.ds(g * UNIT, UNIT), cols])
                back(top.at[g, ch], d, g, ch).wait_recv()
                red[g, d, ch] = (red[g, d, ch].astype(f32) + add).astype(bf16)
                back(red.at[g, d, ch], d - 1, g, ch).start()
        return carry

    lax.fori_loop(1, reach, fold, 0)

    for ch in range(chunks):
        cols = pl.ds(ch * width, width)
        add = dot_rows(own_w, eo[0, pl.ds(0, UNIT), cols])
        for g in range(2):
            back(top.at[g, ch], 0, g, ch).wait_recv()
            add += red[g, 0, ch].astype(f32)
        out[:, cols] = add.astype(bf16)

    def drain(d, carry):
        for g in range(2):
            mlanded(d, g).wait_send()
            for ch in range(chunks):
                landed(d, g, ch).wait_send()
                back(top.at[g, ch], d, g, ch).wait_send()
        return carry

    lax.fori_loop(0, reach, drain, 0)

    def drain_share(d, carry):
        share(d).wait_send()
        return carry

    lax.fori_loop(0, reach + far + 1, drain_share, 0)
    for b in range(reach - 1, reach + 1):
        give(ps.at[0], b).wait_send()
    for j in range(1, far + 1):
        give(psf.at[j - 1], reach + j).wait_send()
        for g in range(2):
            far_send(g, j).wait_send()
            far_back(g, j).wait_send()


def shards(n, reach, chunks, tokens, norm_gain, gate_weight, up_weight, down_weight, chosen, affinity):
    trows, model = tokens.shape
    half = model // 2
    width = half // chunks
    slots = chosen.shape[2]
    hid = gate_weight.shape[2]
    far = n // 2 - reach
    picked = chosen[0]
    weight = jnp.where(picked < trows, affinity[0], 0.0)
    table = jnp.concatenate([picked.astype(f32), weight], axis=0).T
    table = jnp.pad(table, ((0, 0), (0, max(128, 2 * n) - 2 * n)))
    meta = jnp.pad(table, ((0, UNIT - slots), (0, 0)), constant_values=float(trows)).astype(bf16)
    dma, batches = pltpu.SemaphoreType.DMA, reach + far + 1
    vmem = pl.BlockSpec(memory_space=pltpu.VMEM)
    anywhere = pl.BlockSpec(memory_space=pl.ANY)
    return pl.pallas_call(
        functools.partial(kernel, n, reach, slots),
        out_shape=jax.ShapeDtypeStruct((trows, half), bf16),
        in_specs=[vmem] * 3 + [anywhere] * 3,
        out_specs=vmem,
        scratch_shapes=[
            pltpu.VMEM((chunks, trows, width), bf16),
            pltpu.VMEM((2, reach, chunks, trows, width), bf16),
            pltpu.VMEM((2, reach, UNIT, meta.shape[1]), bf16),
            pltpu.VMEM((half, 2 * hid), bf16),
            pltpu.VMEM((half, 2 * hid), bf16),
            pltpu.VMEM((hid, half), bf16),
            pltpu.VMEM((hid, half), bf16),
            pltpu.VMEM((batches, 2 * UNIT, half), bf16),
            pltpu.VMEM((batches, 2 * UNIT, half), bf16),
            pltpu.VMEM((batches, 2 * UNIT, half), bf16),
            pltpu.VMEM((2, 2 * UNIT, half), bf16),
            pltpu.VMEM((2, 2 * UNIT, half), bf16),
            pltpu.VMEM((far, 2 * UNIT, half), bf16),
            pltpu.VMEM((far, 2 * UNIT, half), bf16),
            pltpu.VMEM((2, far, UNIT, half), bf16),
            pltpu.VMEM((2, far, UNIT, half), bf16),
            pltpu.VMEM((2, reach, chunks, trows, width), bf16),
            pltpu.VMEM((2, chunks, trows, width), bf16),
            dma((6,)),
            dma((2, reach, chunks)), dma((2, reach, chunks)),
            dma((2, reach)), dma((2, reach)),
            dma((batches,)), dma((batches,)), dma((batches,)), dma((batches,)),
            dma((2, far)), dma((2, far)), dma((2, far)), dma((2, far)),
            dma((2, reach, chunks)), dma((2, reach, chunks)),
        ],
        compiler_params=pltpu.CompilerParams(
            collective_id=0, has_side_effects=True, vmem_limit_bytes=67043328
        ),
    )(tokens, norm_gain[None, :], meta, gate_weight, up_weight, down_weight)


def solution(mesh):
    n = mesh.shape["ep"]
    in_specs = (
        P(("grp", "ep"), None),
        P(),
        P("ep", None, "tp"),
        P("ep", None, "tp"),
        P("ep", "tp", None),
        P(("grp", "ep"), None, None),
        P(("grp", "ep"), None, None),
    )
    body = functools.partial(shards, n, min(REACH, n // 2 - 1), CHUNKS)
    return jax.shard_map(body, mesh=mesh, in_specs=in_specs, out_specs=P(("grp", "ep"), "tp"), check_vma=False)
```

time: 833 us -> 360 us (0.43)
  blocking collectives: 416 us -> 0 us
  Pallas kernels: 0 us -> 355 us
  waiting for transfers between devices: 296 us -> 0 us
  local copies, waits for them, and re-layouts: 47.6 us -> 1.88 us
  matrix products: 22 us -> 0 us
  starting transfers between devices: 21.9 us -> 0 us
  between operations: 13.5 us -> 0.01 us
    all_to_all x2 -> x0, blocking collectives: 416 us -> none  [the longest x1 407 us: shards(): lax.all_to_all(outgoing, 'ep', split_axis=0, concat_axis=0, tiled=True)]
    pallas_call x0 -> x1, Pallas kernels: none -> 355 us  [shards(): pl.pallas_call(functools.partial(kernel, n, reach, slots), out_shape=jax....]
    all_to_all x1 -> x0, waiting for transfers between devices: 276 us -> none  [shards(): lax.all_to_all(expert_out, 'ep', split_axis=1, concat_axis=1, tiled=True)]
    dot_general x3 -> x0, matrix products: 22 us -> none  [the longest x1 11.6 us: shards(): lax.dot_general(columns, hidden, (((0,), (1,)), ((), ())), preferred_elem...]
    all_to_all x1 -> x0, starting transfers between devices: 21.9 us -> none  [shards(): lax.all_to_all(expert_out, 'ep', split_axis=1, concat_axis=1, tiled=True)]
    all_gather x1 -> x0, waiting for transfers between devices: 20.9 us -> none  [shards(): arrived = lax.all_gather(landed, 'tp', axis=1, tiled=True)]
    gather x2 -> x0, local copies, waits for them, and re-layouts: 14 us -> none  [shards(): outgoing = jnp.take(source, own_slots, axis=0, mode='clip')]
    all_to_all x3 -> x0, local copies, waits for them, and re-layouts: 13.3 us -> none  [the longest x2 10.3 us: shards(): lax.all_to_all(expert_out, 'ep', split_axis=1, concat_axis=1, tiled=True)]
  transfers between devices with their start and end apart: 2 -> 0, of which waited for: 2 -> 0; matrix products, arithmetic and copies ran while one was open for 0% -> 0% of each run, Pallas kernels for 0% -> 0%
where the time goes in v1:
time: 360 us; the launch traced here: 359 us
  Pallas kernels  355 us (99%)
    pallas_call x1, Pallas kernels, shards(): pl.pallas_call(functools.partial(kernel, n, reach, slots), out_shape=jax....  355 us

profile of v1, /device:TPU:37, one launch (start us, length us, event | category | flops | bytes accessed | tf_op | source)
XLA Modules:
  0.0 359.2 jit_solution(2469619374561251480)
XLA Ops:
  0.0 0.7 fusion.3
  0.7 0.7 fusion.4
  1.4 0.1 maximum_bitcast_fusion
  1.5 0.6 fusion.meta
  2.1 355.2 %shard_map.73 = bf16[128,2048]{1,0:T(8,128)(2,1)} custom-call(bf16[128,4096]{1,0:T(8,128)(2,1)} %tokens.1, f32[1,4096]{1,0:T(1,128)} %bitcast.7, bf16[32,128]{1,0:T(8,128)(2,1)} %fusion.meta, bf16[1,4096,384]{2,1,0:T(8,128)(2,1)} %gate_hbm.1, bf16[1,4096,384]{2,1,0:T(8,128)(2,1)} %up_hbm.1, bf16[1,384,4096]{2,1,0:T(8,128)(2,1)} %down_hbm.1), custom_call_target="tpu_custom_call" | custom-call | tf_op jit(solution)/shard_map/pallas_call | solution.py:343
  357.3 1.9 copy.27

commit v2 on v1

v2 whole, which is shorter than its diff:
```python
import functools

import jax
import jax.numpy as jnp
from jax import lax
from jax.experimental import pallas as pl
from jax.experimental.pallas import tpu as pltpu
from jax.sharding import PartitionSpec as P

norm_eps = 1e-06
UNIT = 32
REACH = 11
CHUNKS = 4
f32, bf16 = jnp.float32, jnp.bfloat16


def up8(rows):
    return -(-rows // 8) * 8


def dot(a, b):
    return jnp.dot(a, b, preferred_element_type=f32)


def dot_rows(a, b):
    return lax.dot_general(a, b, (((0,), (0,)), ((), ())), preferred_element_type=f32)


def kernel(
    n, reach, slots, tokens_hbm, gain_hbm, chosen_hbm, affinity_hbm, gate_hbm, up_hbm, down_hbm, out,
    tokens, gain, chosen, affinity, meta, own, ring, mring, w_own, w_oth, d_own, d_oth,
    pk_own, pk_oth, eo, ps, po, far_out, far_got, far_ret, far_in, red, top,
    wsem, dsend, drecv, msend, mrecv, pxs, pxr, pas, par, fs, fr, gs, gr, rs, rr,
):
    me, core = lax.axis_index("ep"), lax.axis_index("tp")
    far = n // 2 - reach
    chunks, trows, width = own.shape
    half = chunks * width
    hid = w_own.shape[1] // 2
    pack_rows = far_out.shape[3]
    end_rows = up8(2 * (slots - slots // 2))
    batches = reach + far + 1
    partner = {"tp": 1 - core}
    sign = (1, -1)

    def at(offset):
        return {"ep": lax.rem(me + offset + n, n)}

    def rcopy(src, dst, s, r, dev):
        return pltpu.make_async_remote_copy(
            src_ref=src, dst_ref=dst, send_sem=s, recv_sem=r, device_id=dev,
            device_id_type=pl.DeviceIdType.MESH,
        )

    def hop(d, g, ch):
        src = own.at[ch] if d is None else ring.at[g, d, ch]
        nxt = 0 if d is None else d + 1
        return rcopy(src, ring.at[g, nxt, ch], dsend.at[g, nxt, ch], drecv.at[g, nxt, ch], at(sign[g]))

    def landed(d, g, ch):
        return rcopy(own.at[ch], ring.at[g, d, ch], dsend.at[g, d, ch], drecv.at[g, d, ch], at(sign[g]))

    def mhop(d, g):
        src = meta if d is None else mring.at[g, d]
        nxt = 0 if d is None else d + 1
        return rcopy(src, mring.at[g, nxt], msend.at[g, nxt], mrecv.at[g, nxt], at(sign[g]))

    def mlanded(d, g):
        return rcopy(meta, mring.at[g, d], msend.at[g, d], mrecv.at[g, d], at(sign[g]))

    def share(d):
        return rcopy(pk_own.at[d], pk_oth.at[d], pxs.at[d], pxr.at[d], partner)

    def give(src, d):
        return rcopy(src, eo.at[d], pas.at[d], par.at[d], partner)

    def far_copy(src, dst, s, r, g, j, h, end, way):
        rows = pl.ds(0, end_rows if end else pack_rows)
        return rcopy(
            src.at[g, j - 1, h, rows], dst.at[g, j - 1, h, rows],
            s.at[g, j - 1, h], r.at[g, j - 1, h], at(way * sign[g] * j),
        )

    def far_send(g, j, h, end):
        return far_copy(far_out, far_got, fs, fr, g, j, h, end, 1)

    def far_back(g, j, h, end):
        return far_copy(far_ret, far_in, gs, gr, g, j, h, end, -1)

    def back(src, d, g, ch):
        return rcopy(src, red.at[g, d, ch], rs.at[g, d, ch], rr.at[g, d, ch], at(-sign[g]))

    lane = lax.broadcasted_iota(jnp.int32, (UNIT, meta.shape[1]), 1)
    tok = lax.broadcasted_iota(jnp.int32, (UNIT, trows), 1).astype(f32)
    slot = lax.broadcasted_iota(jnp.int32, (UNIT, 1), 0)

    def column(m, index):
        return jnp.sum(jnp.where(lane == index, m, 0.0), axis=1, keepdims=True)

    def hot(m, e, weighted):
        value = column(m, n + e) if weighted else 1.0
        return jnp.where(column(m, e) == tok, value, 0.0).astype(bf16)

    pack_r = lax.broadcasted_iota(jnp.int32, (pack_rows, UNIT), 0)
    pack_s = lax.broadcasted_iota(jnp.int32, (pack_rows, UNIT), 1)

    def packer(g, end):
        low = slots // 2
        count = jnp.where(end, low if g == 0 else slots - low, slots)
        first = jnp.where(end, 0 if g == 0 else low, 0)
        a = (pack_r < count) & (pack_s == pack_r + first)
        b = (pack_r >= count) & (pack_r < 2 * count) & (pack_s == pack_r - count + first)
        return [jnp.where(v, 1.0, 0.0).astype(bf16) for v in (a, b)]

    def far_hot(m, g, weighted):
        sides = [[], []]
        for j in range(1, far + 1):
            h = hot(m, lax.rem(me + sign[g] * j + n, n), weighted)
            for side, pk in zip(sides, packer(g, j == far)):
                side.append(dot(pk, h))
        return [jnp.concatenate(side, axis=0).astype(bf16) for side in sides]

    loads = []
    for i, (src, dst) in enumerate((
        (tokens_hbm, tokens),
        (gain_hbm, gain),
        (chosen_hbm.at[0], chosen),
        (affinity_hbm.at[0], affinity),
        (gate_hbm.at[0, pl.ds(core * half, half)], w_own.at[:, pl.ds(0, hid)]),
        (up_hbm.at[0, pl.ds(core * half, half)], w_own.at[:, pl.ds(hid, hid)]),
        (gate_hbm.at[0, pl.ds((1 - core) * half, half)], w_oth.at[:, pl.ds(0, hid)]),
        (up_hbm.at[0, pl.ds((1 - core) * half, half)], w_oth.at[:, pl.ds(hid, hid)]),
        (down_hbm.at[0, :, pl.ds(pl.multiple_of(core * half, 128), half)], d_own),
        (down_hbm.at[0, :, pl.ds(pl.multiple_of((1 - core) * half, 128), half)], d_oth),
    )):
        loads.append(pltpu.make_async_copy(src, dst, wsem.at[i]))
        loads[-1].start()

    barrier = pltpu.get_barrier_semaphore()
    peers = [at(s * j) for j in range(1, far + 1) for s in sign] + [partner]
    for peer in peers:
        pl.semaphore_signal(barrier, inc=1, device_id=peer, device_id_type=pl.DeviceIdType.MESH)

    for buf in (far_got, far_in):
        for g in range(2):
            for h in range(2):
                rest = pl.ds(end_rows, pack_rows - end_rows)
                buf[g, far - 1, h, rest] = jnp.zeros_like(buf[g, far - 1, h, rest])
    loads[0].wait()
    loads[1].wait()
    squares = jnp.zeros((trows, 1), f32)
    for i in range(2 * chunks):
        v = tokens[:, pl.ds(i * width, width)].astype(f32)
        squares += jnp.sum(v * v, axis=1, keepdims=True)
    scale = lax.rsqrt(squares / tokens.shape[1] + norm_eps)
    for ch in range(chunks):
        cols = pl.ds(pl.multiple_of(core * half + ch * width, 128), width)
        own[ch] = (tokens[:, cols].astype(f32) * scale * gain[:, cols]).astype(bf16)
    loads[2].wait()
    loads[3].wait()
    experts = chosen.shape[0]
    spread = lax.broadcasted_iota(jnp.int32, (UNIT, slots), 0) == lax.broadcasted_iota(jnp.int32, (UNIT, slots), 1)
    spread = jnp.where(spread, 1.0, 0.0).astype(bf16)
    e_row = lax.broadcasted_iota(jnp.int32, (experts, meta.shape[1]), 0)
    e_lane = lax.broadcasted_iota(jnp.int32, (experts, meta.shape[1]), 1)
    table = jnp.zeros(meta.shape, f32)
    for ref, shift in ((chosen, 0), (affinity, n)):
        turned = lax.dot_general(
            spread, ref[...].astype(f32).astype(bf16), (((1,), (1,)), ((), ())), preferred_element_type=f32
        )
        place = jnp.where(e_lane == e_row + shift, 1.0, 0.0).astype(bf16)
        table += dot(turned.astype(bf16), place)
    meta[...] = jnp.where(slot < slots, table, float(trows)).astype(bf16)
    pl.semaphore_wait(barrier, len(peers))

    for ch in range(chunks):
        for g in range(2):
            hop(None, g, ch).start()
            if ch == 0:
                mhop(None, g).start()
    pk_own[0, pl.ds(UNIT, UNIT)] = jnp.zeros_like(pk_own[0, pl.ds(UNIT, UNIT)])
    own_hot = hot(meta[...].astype(f32), me, False)
    for ch in range(chunks):
        pk_own[0, pl.ds(0, UNIT), pl.ds(ch * width, width)] = dot(own_hot, own[ch]).astype(bf16)
    share(0).start()
    for load in loads[4:]:
        load.wait()

    def hidden_of(a, b):
        acc = dot(a, w_own[...]) + dot(b, w_oth[...])
        gate, upper = acc[:, :hid], acc[:, hid:]
        return (gate * jax.nn.sigmoid(gate) * upper).astype(bf16)

    def pick(t):
        for g in range(2):
            h = hot(mring[g, t - 1].astype(f32), me, False)
            for ch in range(chunks):
                pk_own[t, pl.ds(g * UNIT, UNIT), pl.ds(ch * width, width)] = dot(h, ring[g, t - 1, ch]).astype(bf16)
        share(t).start()

    def pick_far(h):
        for g in range(2):
            pa, pb = far_hot(mring[g, reach - 1].astype(f32), g, False)
            left = dot(pa, ring[g, reach - 1, 2 * h]) + dot(pb, ring[g, reach - 1, 2 * h + 1])
            for j in range(1, far + 1):
                far_out[g, j - 1, h] = left[(j - 1) * pack_rows : j * pack_rows].astype(bf16)
        for j in range(far, 0, -1):
            for g in range(2):
                far_send(g, j, h, j == far).start()

    def turn(b):
        return jnp.where(b <= reach, b, 2 * reach + far + 1 - b)

    unturn = turn

    def expert(b):
        share(b).wait_recv()
        h = hidden_of(pk_own[b], pk_oth[b])
        spot = lax.rem(turn(b), 2)

        @pl.when(turn(b) >= 2)
        def _():
            give(ps.at[spot], unturn(turn(b) - 2)).wait_send()

        ps[spot] = dot(h, d_oth[...]).astype(bf16)
        give(ps.at[spot], b).start()
        po[spot] = dot(h, d_own[...]).astype(bf16)

    def finish(b):
        give(ps.at[0], b).wait_recv()
        eo[b] = (po[lax.rem(turn(b), 2)].astype(f32) + eo[b].astype(f32)).astype(bf16)

    def step(t, carry):
        @pl.when(t <= reach)
        def _():
            for g in range(2):
                mlanded(t - 1, g).wait_recv()

                @pl.when(t < reach)
                def _():
                    mhop(t - 1, g).start()

        for ch in range(chunks):
            @pl.when(t <= reach)
            def _():
                for g in range(2):
                    landed(t - 1, g, ch).wait_recv()

                    @pl.when(t < reach)
                    def _():
                        hop(t - 1, g, ch).start()

            if ch % 2:
                @pl.when(t == reach)
                def _():
                    pick_far(ch // 2)

            if ch == 0:
                @pl.when(t <= reach + 1)
                def _():
                    expert(t - 1)

            if ch == chunks - 2:
                @pl.when(t >= 2)
                def _():
                    finish(t - 2)

        @pl.when(t <= reach)
        def _():
            pick(t)

        return carry

    lax.fori_loop(1, reach + 3, step, 0)

    def far_step(i, carry):
        j = far - i

        @pl.when(i == 0)
        def _():
            for g in range(2):
                for h in range(2):
                    far_send(g, far, h, True).wait_recv()

        @pl.when((i > 0) & (i < far))
        def _():
            for g in range(2):
                for h in range(2):
                    far_send(g, j, h, False).wait_recv()

        @pl.when(i < far)
        def _():
            for g in range(2):
                pks = packer(g, i == 0)
                for ch in range(chunks):
                    rows = dot_rows(pks[ch % 2], far_got[g, j - 1, ch // 2])
                    pk_own[reach + j, pl.ds(g * UNIT, UNIT), pl.ds(ch * width, width)] = rows.astype(bf16)
            share(reach + j).start()

        @pl.when((i > 0) & (i <= far))
        def _():
            expert(reach + j + 1)

        @pl.when(i > 1)
        def _():
            finish(reach + j + 2)
            for g in range(2):
                pks = packer(g, i == 2)
                for h in range(2):
                    y = dot(pks[0], eo[reach + j + 2, pl.ds(g * UNIT, UNIT), pl.ds(2 * h * width, width)])
                    y += dot(pks[1], eo[reach + j + 2, pl.ds(g * UNIT, UNIT), pl.ds((2 * h + 1) * width, width)])
                    far_ret[g, j + 1, h] = y.astype(bf16)

        @pl.when(i == 2)
        def _():
            for h in range(2):
                for g in range(2):
                    far_back(g, far, h, True).start()

        @pl.when(i > 2)
        def _():
            for g in range(2):
                far_back(g, j + 2, 0, False).start()

        return carry

    lax.fori_loop(0, far + 2, far_step, 0)
    for j in range(far - 1, 0, -1):
        for g in range(2):
            far_back(g, j, 1, False).start()

    own_w = hot(meta[...].astype(f32), me, True)
    near_w = [hot(mring[g, reach - 1].astype(f32), me, True) for g in range(2)]
    far_w = [far_hot(mring[g, reach - 1].astype(f32), g, True) for g in range(2)]
    for h in range(2):
        for j in range(far, 0, -1):
            for g in range(2):
                far_back(g, j, h, j == far).wait_recv()
        for ch in (2 * h, 2 * h + 1):
            cols = pl.ds(ch * width, width)
            for g in range(2):
                total = dot_rows(near_w[g], eo[reach, pl.ds(g * UNIT, UNIT), cols])
                for j in range(1, far + 1):
                    rows = far_w[g][ch % 2][(j - 1) * pack_rows : j * pack_rows]
                    total += dot_rows(rows, far_in[g, j - 1, h])
                top[g, ch] = total.astype(bf16)
                back(top.at[g, ch], reach - 1, g, ch).start()

    def fold(i, carry):
        d = reach - i
        hots = [hot(mring[g, d - 1].astype(f32), me, True) for g in range(2)]
        for ch in range(chunks):
            cols = pl.ds(ch * width, width)
            for g in range(2):
                add = dot_rows(hots[g], eo[d, pl.ds(g * UNIT, UNIT), cols])
                back(top.at[g, ch], d, g, ch).wait_recv()
                red[g, d, ch] = (red[g, d, ch].astype(f32) + add).astype(bf16)
                back(red.at[g, d, ch], d - 1, g, ch).start()
        return carry

    lax.fori_loop(1, reach, fold, 0)

    for ch in range(chunks):
        cols = pl.ds(ch * width, width)
        add = dot_rows(own_w, eo[0, pl.ds(0, UNIT), cols])
        for g in range(2):
            back(top.at[g, ch], 0, g, ch).wait_recv()
            add += red[g, 0, ch].astype(f32)
        out[:, cols] = add.astype(bf16)

    def drain(d, carry):
        for g in range(2):
            mlanded(d, g).wait_send()
            for ch in range(chunks):
                landed(d, g, ch).wait_send()
                back(top.at[g, ch], d, g, ch).wait_send()
        return carry

    lax.fori_loop(0, reach, drain, 0)

    def drain_share(d, carry):
        share(d).wait_send()
        return carry

    lax.fori_loop(0, batches, drain_share, 0)
    for b in (reach + 1, reach + 2) if far > 1 else (reach, reach + 1):
        give(ps.at[0], b).wait_send()
    for j in range(1, far + 1):
        for g in range(2):
            for h in range(2):
                far_send(g, j, h, j == far).wait_send()
                far_back(g, j, h, j == far).wait_send()


def shards(n, reach, chunks, tokens, norm_gain, gate_weight, up_weight, down_weight, chosen, affinity):
    trows, model = tokens.shape
    half = model // 2
    width = half // chunks
    slots = chosen.shape[2]
    hid = gate_weight.shape[2]
    far = n // 2 - reach
    pack_rows = up8(2 * slots)
    lanes = max(128, 2 * n)
    dma, batches = pltpu.SemaphoreType.DMA, reach + far + 1
    vmem = pl.BlockSpec(memory_space=pltpu.VMEM)
    anywhere = pl.BlockSpec(memory_space=pl.ANY)
    return pl.pallas_call(
        functools.partial(kernel, n, reach, slots),
        out_shape=jax.ShapeDtypeStruct((trows, half), bf16),
        in_specs=[anywhere] * 7,
        out_specs=vmem,
        scratch_shapes=[
            pltpu.VMEM((trows, model), bf16),
            pltpu.VMEM((1, model), f32),
            pltpu.VMEM(chosen.shape[1:], jnp.int32),
            pltpu.VMEM(chosen.shape[1:], f32),
            pltpu.VMEM((UNIT, lanes), bf16),
            pltpu.VMEM((chunks, trows, width), bf16),
            pltpu.VMEM((2, reach, chunks, trows, width), bf16),
            pltpu.VMEM((2, reach, UNIT, lanes), bf16),
            pltpu.VMEM((half, 2 * hid), bf16),
            pltpu.VMEM((half, 2 * hid), bf16),
            pltpu.VMEM((hid, half), bf16),
            pltpu.VMEM((hid, half), bf16),
            pltpu.VMEM((batches, 2 * UNIT, half), bf16),
            pltpu.VMEM((batches, 2 * UNIT, half), bf16),
            pltpu.VMEM((batches, 2 * UNIT, half), bf16),
            pltpu.VMEM((2, 2 * UNIT, half), bf16),
            pltpu.VMEM((2, 2 * UNIT, half), bf16),
            pltpu.VMEM((2, far, 2, pack_rows, width), bf16),
            pltpu.VMEM((2, far, 2, pack_rows, width), bf16),
            pltpu.VMEM((2, far, 2, pack_rows, width), bf16),
            pltpu.VMEM((2, far, 2, pack_rows, width), bf16),
            pltpu.VMEM((2, reach, chunks, trows, width), bf16),
            pltpu.VMEM((2, chunks, trows, width), bf16),
            dma((10,)),
            dma((2, reach, chunks)), dma((2, reach, chunks)),
            dma((2, reach)), dma((2, reach)),
            dma((batches,)), dma((batches,)), dma((batches,)), dma((batches,)),
            dma((2, far, 2)), dma((2, far, 2)), dma((2, far, 2)), dma((2, far, 2)),
            dma((2, reach, chunks)), dma((2, reach, chunks)),
        ],
        compiler_params=pltpu.CompilerParams(
            collective_id=0, has_side_effects=True, vmem_limit_bytes=67043328
        ),
    )(tokens, norm_gain[None, :], chosen, affinity, gate_weight, up_weight, down_weight)


def solution(mesh):
    n = mesh.shape["ep"]
    in_specs = (
        P(("grp", "ep"), None),
        P(),
        P("ep", None, "tp"),
        P("ep", None, "tp"),
        P("ep", "tp", None),
        P(("grp", "ep"), None, None),
        P(("grp", "ep"), None, None),
    )
    body = functools.partial(shards, n, min(REACH, n // 2 - 1), CHUNKS)
    return jax.shard_map(body, mesh=mesh, in_specs=in_specs, out_specs=P(("grp", "ep"), "tp"), check_vma=False)
```

time: 360 us -> 342 us (0.950)
  Pallas kernels: 355 us -> 337 us
    pallas_call x1, Pallas kernels: 355 us -> 337 us  [shards(): pl.pallas_call(functools.partial(kernel, n, reach, slots), out_shape=jax....]
where the time goes in v2:
time: 342 us
  Pallas kernels  337 us (99%)
  local copies, waits for them, and re-layouts  4.64 us (1%)
    pallas_call x1, Pallas kernels, shards(): pl.pallas_call(functools.partial(kernel, n, reach, slots), out_shape=jax....  337 us

profile of v2, /device:TPU:37, one launch (start us, length us, event | category | flops | bytes accessed | tf_op | source)
XLA Modules:
  0.0 341.8 jit_solution(16984398496854872784)
XLA Ops:
  0.0 1.4 copy.8.chosen_hbm
  1.4 1.4 copy.9.affinity_hbm
  2.8 337.2 %shard_map.73 = bf16[128,2048]{1,0:T(8,128)(2,1)} custom-call(bf16[128,4096]{1,0:T(8,128)(2,1)} %tokens_hbm.1, f32[1,4096]{1,0:T(1,128)} %bitcast.1, s32[1,32,20]{2,1,0:T(8,128)} %copy.8.chosen_hbm, f32[1,32,20]{2,1,0:T(8,128)} %copy.9.affinity_hbm, bf16[1,4096,384]{2,1,0:T(8,128)(2,1)} %gate_hbm.1, bf16[1,4096,384]{2,1,0:T(8,128)(2,1)} %up_hbm.1, ...), custom_call_target="tpu_custom_call" | custom-call | tf_op jit(solution)/shard_map/pallas_call | solution.py:407
  340.0 1.9 copy.11

commit v3 on v2

--- a/solution.py
+++ b/solution.py
@@ -29,7 +29,7 @@
 def kernel(
     n, reach, slots, tokens_hbm, gain_hbm, chosen_hbm, affinity_hbm, gate_hbm, up_hbm, down_hbm, out,
     tokens, gain, chosen, affinity, meta, own, ring, mring, w_own, w_oth, d_own, d_oth,
-    pk_own, pk_oth, eo, ps, po, far_out, far_got, far_ret, far_in, red, top,
+    pk_own, pk_oth, eo, ps, po, psf, pof, far_out, far_got, far_ret, far_in, red, top,
     wsem, dsend, drecv, msend, mrecv, pxs, pxr, pas, par, fs, fr, gs, gr, rs, rr,
 ):
     me, core = lax.axis_index("ep"), lax.axis_index("tp")
@@ -38,7 +38,6 @@
     half = chunks * width
     hid = w_own.shape[1] // 2
     pack_rows = far_out.shape[3]
-    end_rows = up8(2 * (slots - slots // 2))
     batches = reach + far + 1
     partner = {"tp": 1 - core}
     sign = (1, -1)
@@ -74,18 +73,19 @@
     def give(src, d):
         return rcopy(src, eo.at[d], pas.at[d], par.at[d], partner)
 
-    def far_copy(src, dst, s, r, g, j, h, end, way):
-        rows = pl.ds(0, end_rows if end else pack_rows)
+    def far_copy(src, dst, s, r, g, j, h, way):
         return rcopy(
-            src.at[g, j - 1, h, rows], dst.at[g, j - 1, h, rows],
-            s.at[g, j - 1, h], r.at[g, j - 1, h], at(way * sign[g] * j),
+            src.at[g, h, j - 1], dst.at[g, h, j - 1], s.at[g, h, j - 1], r.at[g, h, j - 1], at(way * sign[g] * j)
         )
 
-    def far_send(g, j, h, end):
-        return far_copy(far_out, far_got, fs, fr, g, j, h, end, 1)
-
-    def far_back(g, j, h, end):
-        return far_copy(far_ret, far_in, gs, gr, g, j, h, end, -1)
+    def far_send(g, j, h):
+        return far_copy(far_out, far_got, fs, fr, g, j, h, 1)
+
+    def far_back(g, j, h):
+        return far_copy(far_ret, far_in, gs, gr, g, j, h, -1)
+
+    def parts_of(j):
+        return (0,) if j == far else (0, 1)
 
     def back(src, d, g, ch):
         return rcopy(src, red.at[g, d, ch], rs.at[g, d, ch], rr.at[g, d, ch], at(-sign[g]))
@@ -104,28 +104,33 @@
     pack_r = lax.broadcasted_iota(jnp.int32, (pack_rows, UNIT), 0)
     pack_s = lax.broadcasted_iota(jnp.int32, (pack_rows, UNIT), 1)
 
-    def packer(g, end):
+    def packer(g, end, ch):
         low = slots // 2
-        count = jnp.where(end, low if g == 0 else slots - low, slots)
-        first = jnp.where(end, 0 if g == 0 else low, 0)
-        a = (pack_r < count) & (pack_s == pack_r + first)
-        b = (pack_r >= count) & (pack_r < 2 * count) & (pack_s == pack_r - count + first)
-        return [jnp.where(v, 1.0, 0.0).astype(bf16) for v in (a, b)]
+        count, first, place = slots, 0, ch % 2
+        if end:
+            count, first, place = (low, 0, ch) if g == 0 else (slots - low, low, ch)
+        local = pack_r - place * count
+        keep = (local >= 0) & (local < count) & (pack_s == local + first)
+        return jnp.where(keep, 1.0, 0.0).astype(bf16)
+
+    def part(j, ch):
+        return 0 if j == far else ch // 2
 
     def far_hot(m, g, weighted):
-        sides = [[], []]
-        for j in range(1, far + 1):
-            h = hot(m, lax.rem(me + sign[g] * j + n, n), weighted)
-            for side, pk in zip(sides, packer(g, j == far)):
-                side.append(dot(pk, h))
-        return [jnp.concatenate(side, axis=0).astype(bf16) for side in sides]
+        hots = [hot(m, lax.rem(me + sign[g] * j + n, n), weighted) for j in range(1, far + 1)]
+        sides = []
+        for ch in range(2 if far > 1 else 0):
+            pk = packer(g, False, ch)
+            sides.append(jnp.concatenate([dot(pk, h) for h in hots[:-1]], axis=0).astype(bf16))
+        ends = [dot(packer(g, True, ch), hots[-1]).astype(bf16) for ch in range(chunks)]
+        return sides, ends
 
     loads = []
     for i, (src, dst) in enumerate((
         (tokens_hbm, tokens),
         (gain_hbm, gain),
-        (chosen_hbm.at[0], chosen),
-        (affinity_hbm.at[0], affinity),
+        (chosen_hbm, chosen),
+        (affinity_hbm, affinity),
         (gate_hbm.at[0, pl.ds(core * half, half)], w_own.at[:, pl.ds(0, hid)]),
         (up_hbm.at[0, pl.ds(core * half, half)], w_own.at[:, pl.ds(hid, hid)]),
         (gate_hbm.at[0, pl.ds((1 - core) * half, half)], w_oth.at[:, pl.ds(0, hid)]),
@@ -137,15 +142,10 @@
         loads[-1].start()
 
     barrier = pltpu.get_barrier_semaphore()
-    peers = [at(s * j) for j in range(1, far + 1) for s in sign] + [partner]
+    peers = [at(1), at(-1), partner]
     for peer in peers:
         pl.semaphore_signal(barrier, inc=1, device_id=peer, device_id_type=pl.DeviceIdType.MESH)
 
-    for buf in (far_got, far_in):
-        for g in range(2):
-            for h in range(2):
-                rest = pl.ds(end_rows, pack_rows - end_rows)
-                buf[g, far - 1, h, rest] = jnp.zeros_like(buf[g, far - 1, h, rest])
     loads[0].wait()
     loads[1].wait()
     squares = jnp.zeros((trows, 1), f32)
@@ -158,18 +158,16 @@
         own[ch] = (tokens[:, cols].astype(f32) * scale * gain[:, cols]).astype(bf16)
     loads[2].wait()
     loads[3].wait()
-    experts = chosen.shape[0]
+    experts = chosen.shape[2]
     spread = lax.broadcasted_iota(jnp.int32, (UNIT, slots), 0) == lax.broadcasted_iota(jnp.int32, (UNIT, slots), 1)
     spread = jnp.where(spread, 1.0, 0.0).astype(bf16)
     e_row = lax.broadcasted_iota(jnp.int32, (experts, meta.shape[1]), 0)
     e_lane = lax.broadcasted_iota(jnp.int32, (experts, meta.shape[1]), 1)
-    table = jnp.zeros(meta.shape, f32)
+    table = jnp.zeros((slots, meta.shape[1]), f32)
     for ref, shift in ((chosen, 0), (affinity, n)):
-        turned = lax.dot_general(
-            spread, ref[...].astype(f32).astype(bf16), (((1,), (1,)), ((), ())), preferred_element_type=f32
-        )
         place = jnp.where(e_lane == e_row + shift, 1.0, 0.0).astype(bf16)
-        table += dot(turned.astype(bf16), place)
+        table += dot(ref[:, 0, :].astype(f32).astype(bf16), place)
+    table = dot(spread, table.astype(bf16))
     meta[...] = jnp.where(slot < slots, table, float(trows)).astype(bf16)
     pl.semaphore_wait(barrier, len(peers))
 
@@ -200,27 +198,28 @@
 
     def pick_far(h):
         for g in range(2):
-            pa, pb = far_hot(mring[g, reach - 1].astype(f32), g, False)
-            left = dot(pa, ring[g, reach - 1, 2 * h]) + dot(pb, ring[g, reach - 1, 2 * h + 1])
-            for j in range(1, far + 1):
-                far_out[g, j - 1, h] = left[(j - 1) * pack_rows : j * pack_rows].astype(bf16)
-        for j in range(far, 0, -1):
-            for g in range(2):
-                far_send(g, j, h, j == far).start()
-
-    def turn(b):
-        return jnp.where(b <= reach, b, 2 * reach + far + 1 - b)
-
-    unturn = turn
+            sides, ends = far_hot(mring[g, reach - 1].astype(f32), g, False)
+            if far > 1:
+                y = dot(sides[0], ring[g, reach - 1, 2 * h]) + dot(sides[1], ring[g, reach - 1, 2 * h + 1])
+                far_out[g, h, pl.ds(0, far - 1)] = y.astype(bf16).reshape(far - 1, pack_rows, width)
+            if h == 1:
+                y = sum(dot(ends[ch], ring[g, reach - 1, ch]) for ch in range(chunks))
+                far_out[g, 0, far - 1] = y.astype(bf16)
+        first = [(far - 1, 0)] if far > 1 else []
+        rest = [(far, 0)] + ([(far - 1, 1)] if far > 1 else [])
+        rest += [(j, p) for j in range(far - 2, 0, -1) for p in (0, 1)]
+        for j, p in rest if h else first:
+            for g in range(2):
+                far_send(g, j, p).start()
 
     def expert(b):
         share(b).wait_recv()
         h = hidden_of(pk_own[b], pk_oth[b])
-        spot = lax.rem(turn(b), 2)
-
-        @pl.when(turn(b) >= 2)
+        spot = lax.rem(b, 2)
+
+        @pl.when(b >= 2)
         def _():
-            give(ps.at[spot], unturn(turn(b) - 2)).wait_send()
+            give(ps.at[spot], b - 2).wait_send()
 
         ps[spot] = dot(h, d_oth[...]).astype(bf16)
         give(ps.at[spot], b).start()
@@ -228,7 +227,7 @@
 
     def finish(b):
         give(ps.at[0], b).wait_recv()
-        eo[b] = (po[lax.rem(turn(b), 2)].astype(f32) + eo[b].astype(f32)).astype(bf16)
+        eo[b] = (po[lax.rem(b, 2)].astype(f32) + eo[b].astype(f32)).astype(bf16)
 
     def step(t, carry):
         @pl.when(t <= reach)
@@ -273,76 +272,64 @@
 
     lax.fori_loop(1, reach + 3, step, 0)
 
-    def far_step(i, carry):
-        j = far - i
-
-        @pl.when(i == 0)
-        def _():
-            for g in range(2):
-                for h in range(2):
-                    far_send(g, far, h, True).wait_recv()
-
-        @pl.when((i > 0) & (i < far))
-        def _():
-            for g in range(2):
-                for h in range(2):
-                    far_send(g, j, h, False).wait_recv()
-
-        @pl.when(i < far)
-        def _():
-            for g in range(2):
-                pks = packer(g, i == 0)
+    def far_group(js):
+        for j in js:
+            for g in range(2):
+                for p in parts_of(j):
+                    far_send(g, j, p).wait_recv()
+            for g in range(2):
                 for ch in range(chunks):
-                    rows = dot_rows(pks[ch % 2], far_got[g, j - 1, ch // 2])
+                    rows = dot_rows(packer(g, j == far, ch), far_got[g, part(j, ch), j - 1])
                     pk_own[reach + j, pl.ds(g * UNIT, UNIT), pl.ds(ch * width, width)] = rows.astype(bf16)
             share(reach + j).start()
-
-        @pl.when((i > 0) & (i <= far))
-        def _():
-            expert(reach + j + 1)
-
-        @pl.when(i > 1)
-        def _():
-            finish(reach + j + 2)
-            for g in range(2):
-                pks = packer(g, i == 2)
-                for h in range(2):
-                    y = dot(pks[0], eo[reach + j + 2, pl.ds(g * UNIT, UNIT), pl.ds(2 * h * width, width)])
-                    y += dot(pks[1], eo[reach + j + 2, pl.ds(g * UNIT, UNIT), pl.ds((2 * h + 1) * width, width)])
-                    far_ret[g, j + 1, h] = y.astype(bf16)
-
-        @pl.when(i == 2)
-        def _():
-            for h in range(2):
+        for j in js:
+            share(reach + j).wait_recv()
+        low, count = min(js), len(js)
+        group, rows = pl.ds(reach + low, count), count * 2 * UNIT
+        h = hidden_of(pk_own[group].reshape(rows, half), pk_oth[group].reshape(rows, half))
+        spots = pl.ds(low - 1, count)
+        psf[spots] = dot(h, d_oth[...]).astype(bf16).reshape(count, 2 * UNIT, half)
+        for j in js:
+            give(psf.at[j - 1], reach + j).start()
+        pof[spots] = dot(h, d_own[...]).astype(bf16).reshape(count, 2 * UNIT, half)
+        for j in js:
+            b = reach + j
+            give(psf.at[j - 1], b).wait_recv()
+            eo[b] = (pof[j - 1].astype(f32) + eo[b].astype(f32)).astype(bf16)
+            for g in range(2):
+                for p in parts_of(j):
+                    y = jnp.zeros((pack_rows, width), f32)
+                    for ch in range(chunks):
+                        if part(j, ch) == p:
+                            y += dot(packer(g, j == far, ch), eo[b, pl.ds(g * UNIT, UNIT), pl.ds(ch * width, width)])
+                    far_ret[g, p, j - 1] = y.astype(bf16)
+                far_back(g, j, 0).start()
+        for j in js:
+            if j != far:
                 for g in range(2):
-                    far_back(g, far, h, True).start()
-
-        @pl.when(i > 2)
-        def _():
-            for g in range(2):
-                far_back(g, j + 2, 0, False).start()
-
-        return carry
-
-    lax.fori_loop(0, far + 2, far_step, 0)
-    for j in range(far - 1, 0, -1):
-        for g in range(2):
-            far_back(g, j, 1, False).start()
+                    far_back(g, j, 1).start()
+
+    order = list(range(far, 0, -1))
+    far_group(order[:2])
+    if far > 2:
+        far_group(order[2:])
 
     own_w = hot(meta[...].astype(f32), me, True)
     near_w = [hot(mring[g, reach - 1].astype(f32), me, True) for g in range(2)]
     far_w = [far_hot(mring[g, reach - 1].astype(f32), g, True) for g in range(2)]
     for h in range(2):
-        for j in range(far, 0, -1):
-            for g in range(2):
-                far_back(g, j, h, j == far).wait_recv()
+        for j in order:
+            if h in parts_of(j):
+                for g in range(2):
+                    far_back(g, j, h).wait_recv()
         for ch in (2 * h, 2 * h + 1):
             cols = pl.ds(ch * width, width)
             for g in range(2):
+                sides, ends = far_w[g]
                 total = dot_rows(near_w[g], eo[reach, pl.ds(g * UNIT, UNIT), cols])
-                for j in range(1, far + 1):
-                    rows = far_w[g][ch % 2][(j - 1) * pack_rows : j * pack_rows]
-                    total += dot_rows(rows, far_in[g, j - 1, h])
+                total += dot_rows(ends[ch], far_in[g, 0, far - 1])
+                if far > 1:
+                    total += dot_rows(sides[ch % 2], far_in[g, h, pl.ds(0, far - 1)].reshape((far - 1) * pack_rows, width))
                 top[g, ch] = total.astype(bf16)
                 back(top.at[g, ch], reach - 1, g, ch).start()
 
@@ -383,13 +370,14 @@
         return carry
 
     lax.fori_loop(0, batches, drain_share, 0)
-    for b in (reach + 1, reach + 2) if far > 1 else (reach, reach + 1):
+    for b in (reach - 1, reach):
         give(ps.at[0], b).wait_send()
-    for j in range(1, far + 1):
-        for g in range(2):
-            for h in range(2):
-                far_send(g, j, h, j == far).wait_send()
-                far_back(g, j, h, j == far).wait_send()
+    for j in order:
+        give(psf.at[j - 1], reach + j).wait_send()
+        for g in range(2):
+            for p in parts_of(j):
+                far_send(g, j, p).wait_send()
+                far_back(g, j, p).wait_send()
 
 
 def shards(n, reach, chunks, tokens, norm_gain, gate_weight, up_weight, down_weight, chosen, affinity):
@@ -399,7 +387,8 @@
     slots = chosen.shape[2]
     hid = gate_weight.shape[2]
     far = n // 2 - reach
-    pack_rows = up8(2 * slots)
+    pack_rows = up8(max(2 * slots, 4 * (slots - slots // 2)))
+    chosen, affinity = [jnp.transpose(v, (2, 0, 1)) for v in (chosen, affinity)]
     lanes = max(128, 2 * n)
     dma, batches = pltpu.SemaphoreType.DMA, reach + far + 1
     vmem = pl.BlockSpec(memory_space=pltpu.VMEM)
@@ -412,8 +401,8 @@
         scratch_shapes=[
             pltpu.VMEM((trows, model), bf16),
             pltpu.VMEM((1, model), f32),
-            pltpu.VMEM(chosen.shape[1:], jnp.int32),
-            pltpu.VMEM(chosen.shape[1:], f32),
+            pltpu.VMEM(chosen.shape, jnp.int32),
+            pltpu.VMEM(chosen.shape, f32),
             pltpu.VMEM((UNIT, lanes), bf16),
             pltpu.VMEM((chunks, trows, width), bf16),
             pltpu.VMEM((2, reach, chunks, trows, width), bf16),
@@ -427,17 +416,19 @@
             pltpu.VMEM((batches, 2 * UNIT, half), bf16),
             pltpu.VMEM((2, 2 * UNIT, half), bf16),
             pltpu.VMEM((2, 2 * UNIT, half), bf16),
-            pltpu.VMEM((2, far, 2, pack_rows, width), bf16),
-            pltpu.VMEM((2, far, 2, pack_rows, width), bf16),
-            pltpu.VMEM((2, far, 2, pack_rows, width), bf16),
-            pltpu.VMEM((2, far, 2, pack_rows, width), bf16),
+            pltpu.VMEM((far, 2 * UNIT, half), bf16),
+            pltpu.VMEM((far, 2 * UNIT, half), bf16),
+            pltpu.VMEM((2, 2, far, pack_rows, width), bf16),
+            pltpu.VMEM((2, 2, far, pack_rows, width), bf16),
+            pltpu.VMEM((2, 2, far, pack_rows, width), bf16),
+            pltpu.VMEM((2, 2, far, pack_rows, width), bf16),
             pltpu.VMEM((2, reach, chunks, trows, width), bf16),
             pltpu.VMEM((2, chunks, trows, width), bf16),
             dma((10,)),
             dma((2, reach, chunks)), dma((2, reach, chunks)),
             dma((2, reach)), dma((2, reach)),
             dma((batches,)), dma((batches,)), dma((batches,)), dma((batches,)),
-            dma((2, far, 2)), dma((2, far, 2)), dma((2, far, 2)), dma((2, far, 2)),
+            dma((2, 2, far)), dma((2, 2, far)), dma((2, 2, far)), dma((2, 2, far)),
             dma((2, reach, chunks)), dma((2, reach, chunks)),
         ],
         compiler_params=pltpu.CompilerParams(

time: 342 us -> 335 us (0.980)
  Pallas kernels: 337 us -> 332 us
    pallas_call x1, Pallas kernels: 337 us -> 332 us  [shards(): pl.pallas_call(functools.partial(kernel, n, reach, slots), out_shape=jax....]
where the time goes in v3:
time: 335 us; the launch traced here: 334 us
  Pallas kernels  332 us (99%)
    pallas_call x1, Pallas kernels, shards(): pl.pallas_call(functools.partial(kernel, n, reach, slots), out_shape=jax....  332 us

profile of v3, /device:TPU:37, one launch (start us, length us, event | category | flops | bytes accessed | tf_op | source)
XLA Modules:
  0.0 334.2 jit_solution(6039543364726859531)
XLA Ops:
  0.0 332.3 %shard_map.73 = bf16[128,2048]{1,0:T(8,128)(2,1)} custom-call(bf16[128,4096]{1,0:T(8,128)(2,1)} %tokens_hbm.1, f32[1,4096]{1,0:T(1,128)} %bitcast.3, s32[20,1,32]{2,1,0:T(1,128)} %bitcast.4, f32[20,1,32]{2,1,0:T(1,128)} %bitcast.5, bf16[1,4096,384]{2,1,0:T(8,128)(2,1)} %gate_hbm.1, bf16[1,4096,384]{2,1,0:T(8,128)(2,1)} %up_hbm.1, bf16[1,384,4096]{2,1,0:T(8,128)(2,1)} %down_hbm.1), custom_call_target="tpu_custom_call" | custom-call | tf_op jit(solution)/shard_map/pallas_call | solution.py:396
  332.3 1.9 copy.9

commit v4 on v3

--- a/solution.py
+++ b/solution.py
@@ -9,7 +9,7 @@
 
 norm_eps = 1e-06
 UNIT = 32
-REACH = 11
+REACH = 10
 CHUNKS = 4
 f32, bf16 = jnp.float32, jnp.bfloat16
 
@@ -90,12 +90,13 @@
     def back(src, d, g, ch):
         return rcopy(src, red.at[g, d, ch], rs.at[g, d, ch], rr.at[g, d, ch], at(-sign[g]))
 
-    lane = lax.broadcasted_iota(jnp.int32, (UNIT, meta.shape[1]), 1)
+    low = slots // 2
+    lane = lax.broadcasted_iota(jnp.int32, meta.shape, 1)
     tok = lax.broadcasted_iota(jnp.int32, (UNIT, trows), 1).astype(f32)
-    slot = lax.broadcasted_iota(jnp.int32, (UNIT, 1), 0)
 
     def column(m, index):
-        return jnp.sum(jnp.where(lane == index, m, 0.0), axis=1, keepdims=True)
+        pair = [jnp.sum(jnp.where(lane == index + 2 * n * i, m, 0.0), axis=1, keepdims=True) for i in range(2)]
+        return jnp.concatenate(pair, axis=0)
 
     def hot(m, e, weighted):
         value = column(m, n + e) if weighted else 1.0
@@ -105,12 +106,13 @@
     pack_s = lax.broadcasted_iota(jnp.int32, (pack_rows, UNIT), 1)
 
     def packer(g, end, ch):
-        low = slots // 2
         count, first, place = slots, 0, ch % 2
         if end:
             count, first, place = (low, 0, ch) if g == 0 else (slots - low, low, ch)
         local = pack_r - place * count
-        keep = (local >= 0) & (local < count) & (pack_s == local + first)
+        wanted = local + first
+        wanted = jnp.where(wanted < low, wanted, wanted - low + UNIT // 2)
+        keep = (local >= 0) & (local < count) & (pack_s == wanted)
         return jnp.where(keep, 1.0, 0.0).astype(bf16)
 
     def part(j, ch):
@@ -159,16 +161,20 @@
     loads[2].wait()
     loads[3].wait()
     experts = chosen.shape[2]
-    spread = lax.broadcasted_iota(jnp.int32, (UNIT, slots), 0) == lax.broadcasted_iota(jnp.int32, (UNIT, slots), 1)
-    spread = jnp.where(spread, 1.0, 0.0).astype(bf16)
+    s_row = lax.broadcasted_iota(jnp.int32, (meta.shape[0], slots), 0)
+    s_col = lax.broadcasted_iota(jnp.int32, (meta.shape[0], slots), 1)
     e_row = lax.broadcasted_iota(jnp.int32, (experts, meta.shape[1]), 0)
     e_lane = lax.broadcasted_iota(jnp.int32, (experts, meta.shape[1]), 1)
-    table = jnp.zeros((slots, meta.shape[1]), f32)
-    for ref, shift in ((chosen, 0), (affinity, n)):
-        place = jnp.where(e_lane == e_row + shift, 1.0, 0.0).astype(bf16)
-        table += dot(ref[:, 0, :].astype(f32).astype(bf16), place)
-    table = dot(spread, table.astype(bf16))
-    meta[...] = jnp.where(slot < slots, table, float(trows)).astype(bf16)
+    table = jnp.zeros(meta.shape, f32)
+    for i, (first, count) in enumerate(((0, low), (low, slots - low))):
+        spread = jnp.where((s_row < count) & (s_col == s_row + first), 1.0, 0.0).astype(bf16)
+        dead = lax.broadcasted_iota(jnp.int32, meta.shape, 0) >= count
+        table += jnp.where(dead & (lane >= 2 * n * i) & (lane < 2 * n * i + n), float(trows), 0.0)
+        for ref, shift in ((chosen, 0), (affinity, n)):
+            place = jnp.where(e_lane == e_row + shift + 2 * n * i, 1.0, 0.0).astype(bf16)
+            moved = dot(ref[:, 0, :].astype(f32).astype(bf16), place).astype(bf16)
+            table += dot(spread, moved)
+    meta[...] = table.astype(bf16)
     pl.semaphore_wait(barrier, len(peers))
 
     for ch in range(chunks):
@@ -272,7 +278,7 @@
 
     lax.fori_loop(1, reach + 3, step, 0)
 
-    def far_group(js):
+    def far_arrive(js):
         for j in js:
             for g in range(2):
                 for p in parts_of(j):
@@ -282,12 +288,14 @@
                     rows = dot_rows(packer(g, j == far, ch), far_got[g, part(j, ch), j - 1])
                     pk_own[reach + j, pl.ds(g * UNIT, UNIT), pl.ds(ch * width, width)] = rows.astype(bf16)
             share(reach + j).start()
+
+    def far_experts(js):
         for j in js:
             share(reach + j).wait_recv()
-        low, count = min(js), len(js)
-        group, rows = pl.ds(reach + low, count), count * 2 * UNIT
+        least, count = min(js), len(js)
+        group, rows = pl.ds(reach + least, count), count * 2 * UNIT
         h = hidden_of(pk_own[group].reshape(rows, half), pk_oth[group].reshape(rows, half))
-        spots = pl.ds(low - 1, count)
+        spots = pl.ds(least - 1, count)
         psf[spots] = dot(h, d_oth[...]).astype(bf16).reshape(count, 2 * UNIT, half)
         for j in js:
             give(psf.at[j - 1], reach + j).start()
@@ -303,16 +311,23 @@
                         if part(j, ch) == p:
                             y += dot(packer(g, j == far, ch), eo[b, pl.ds(g * UNIT, UNIT), pl.ds(ch * width, width)])
                     far_ret[g, p, j - 1] = y.astype(bf16)
-                far_back(g, j, 0).start()
-        for j in js:
-            if j != far:
-                for g in range(2):
-                    far_back(g, j, 1).start()
+
+    def far_return(js):
+        for p in range(2):
+            for j in js:
+                if p in parts_of(j):
+                    for g in range(2):
+                        far_back(g, j, p).start()
 
     order = list(range(far, 0, -1))
-    far_group(order[:2])
-    if far > 2:
-        far_group(order[2:])
+    outer, inner = order[:2], order[2:]
+    far_arrive(outer)
+    far_experts(outer)
+    far_arrive(inner)
+    far_return(outer)
+    if inner:
+        far_experts(inner)
+        far_return(inner)
 
     own_w = hot(meta[...].astype(f32), me, True)
     near_w = [hot(mring[g, reach - 1].astype(f32), me, True) for g in range(2)]
@@ -389,7 +404,7 @@
     far = n // 2 - reach
     pack_rows = up8(max(2 * slots, 4 * (slots - slots // 2)))
     chosen, affinity = [jnp.transpose(v, (2, 0, 1)) for v in (chosen, affinity)]
-    lanes = max(128, 2 * n)
+    lanes = max(128, 4 * n)
     dma, batches = pltpu.SemaphoreType.DMA, reach + far + 1
     vmem = pl.BlockSpec(memory_space=pltpu.VMEM)
     anywhere = pl.BlockSpec(memory_space=pl.ANY)
@@ -403,10 +418,10 @@
             pltpu.VMEM((1, model), f32),
             pltpu.VMEM(chosen.shape, jnp.int32),
             pltpu.VMEM(chosen.shape, f32),
-            pltpu.VMEM((UNIT, lanes), bf16),
+            pltpu.VMEM((UNIT // 2, lanes), bf16),
             pltpu.VMEM((chunks, trows, width), bf16),
             pltpu.VMEM((2, reach, chunks, trows, width), bf16),
-            pltpu.VMEM((2, reach, UNIT, lanes), bf16),
+            pltpu.VMEM((2, reach, UNIT // 2, lanes), bf16),
             pltpu.VMEM((half, 2 * hid), bf16),
             pltpu.VMEM((half, 2 * hid), bf16),
             pltpu.VMEM((hid, half), bf16),

time: 335 us -> 328 us (0.979)
  Pallas kernels: 332 us -> 326 us
    pallas_call x1, Pallas kernels: 332 us -> 326 us  [shards(): pl.pallas_call(functools.partial(kernel, n, reach, slots), out_shape=jax....]
where the time goes in v4:
time: 328 us
  Pallas kernels  326 us (99%)
    pallas_call x1, Pallas kernels, shards(): pl.pallas_call(functools.partial(kernel, n, reach, slots), out_shape=jax....  326 us

profile of v4, /device:TPU:37, one launch (start us, length us, event | category | flops | bytes accessed | tf_op | source)
XLA Modules:
  0.0 327.8 jit_solution(7251522698548835813)
XLA Ops:
  0.0 325.9 %shard_map.73 = bf16[128,2048]{1,0:T(8,128)(2,1)} custom-call(bf16[128,4096]{1,0:T(8,128)(2,1)} %tokens_hbm.1, f32[1,4096]{1,0:T(1,128)} %bitcast.3, s32[20,1,32]{2,1,0:T(1,128)} %bitcast.4, f32[20,1,32]{2,1,0:T(1,128)} %bitcast.5, bf16[1,4096,384]{2,1,0:T(8,128)(2,1)} %gate_hbm.1, bf16[1,4096,384]{2,1,0:T(8,128)(2,1)} %up_hbm.1, bf16[1,384,4096]{2,1,0:T(8,128)(2,1)} %down_hbm.1), custom_call_target="tpu_custom_call" | custom-call | tf_op jit(solution)/shard_map/pallas_call | solution.py:411
  325.9 1.9 copy.9

commit v5 on v4

--- a/solution.py
+++ b/solution.py
@@ -323,8 +323,11 @@
     outer, inner = order[:2], order[2:]
     far_arrive(outer)
     far_experts(outer)
-    far_arrive(inner)
-    far_return(outer)
+    early = inner[:max(len(inner) - 2, 0)]
+    far_arrive(early)
+    far_return(outer[:1])
+    far_arrive(inner[len(early):])
+    far_return(outer[1:])
     if inner:
         far_experts(inner)
         far_return(inner)
@@ -410,7 +413,7 @@
     anywhere = pl.BlockSpec(memory_space=pl.ANY)
     return pl.pallas_call(
         functools.partial(kernel, n, reach, slots),
-        out_shape=jax.ShapeDtypeStruct((trows, half), bf16),
+        out_shape=pltpu.VMEM((trows, half), bf16),
         in_specs=[anywhere] * 7,
         out_specs=vmem,
         scratch_shapes=[
@@ -447,7 +450,7 @@
             dma((2, reach, chunks)), dma((2, reach, chunks)),
         ],
         compiler_params=pltpu.CompilerParams(
-            collective_id=0, has_side_effects=True, vmem_limit_bytes=67043328
+            collective_id=0, has_side_effects=True, vmem_limit_bytes=58 * 2**20
         ),
     )(tokens, norm_gain[None, :], chosen, affinity, gate_weight, up_weight, down_weight)
 

time: 328 us -> 328 us (level)
  no operation moved by 1% of the time
where the time goes in v5:
time: 328 us
  Pallas kernels  327 us (100%)
    pallas_call x1, Pallas kernels, shards(): pl.pallas_call(functools.partial(kernel, n, reach, slots), out_shape=pltp...  327 us

profile of v5, /device:TPU:37, one launch (start us, length us, event | category | flops | bytes accessed | tf_op | source)
XLA Modules:
  0.0 327.6 jit_solution(6522775574089887915)
XLA Ops:
  0.0 326.8 %shard_map.73 = bf16[128,2048]{1,0:T(8,128)(2,1)S(1)} custom-call(bf16[128,4096]{1,0:T(8,128)(2,1)} %tokens_hbm.1, f32[1,4096]{1,0:T(1,128)} %bitcast.3, s32[20,1,32]{2,1,0:T(1,128)} %bitcast.4, f32[20,1,32]{2,1,0:T(1,128)} %bitcast.5, bf16[1,4096,384]{2,1,0:T(8,128)(2,1)} %gate_hbm.1, bf16[1,4096,384]{2,1,0:T(8,128)(2,1)} %up_hbm.1, ...), custom_call_target="tpu_custom_call" | custom-call | tf_op jit(solution)/shard_map/pallas_call | solution.py:414
  326.8 0.8 copy.9

commit v6 on v5

--- a/solution.py
+++ b/solution.py
@@ -127,6 +127,11 @@
         ends = [dot(packer(g, True, ch), hots[-1]).astype(bf16) for ch in range(chunks)]
         return sides, ends
 
+    barrier = pltpu.get_barrier_semaphore()
+    peers = [at(1), at(-1), partner]
+    for peer in peers:
+        pl.semaphore_signal(barrier, inc=1, device_id=peer, device_id_type=pl.DeviceIdType.MESH)
+
     loads = []
     for i, (src, dst) in enumerate((
         (tokens_hbm, tokens),
@@ -142,11 +147,6 @@
     )):
         loads.append(pltpu.make_async_copy(src, dst, wsem.at[i]))
         loads[-1].start()
-
-    barrier = pltpu.get_barrier_semaphore()
-    peers = [at(1), at(-1), partner]
-    for peer in peers:
-        pl.semaphore_signal(barrier, inc=1, device_id=peer, device_id_type=pl.DeviceIdType.MESH)
 
     loads[0].wait()
     loads[1].wait()
@@ -312,25 +312,22 @@
                             y += dot(packer(g, j == far, ch), eo[b, pl.ds(g * UNIT, UNIT), pl.ds(ch * width, width)])
                     far_ret[g, p, j - 1] = y.astype(bf16)
 
-    def far_return(js):
-        for p in range(2):
-            for j in js:
-                if p in parts_of(j):
-                    for g in range(2):
-                        far_back(g, j, p).start()
+    def far_return(js, p):
+        for j in js:
+            if p in parts_of(j):
+                for g in range(2):
+                    far_back(g, j, p).start()
 
     order = list(range(far, 0, -1))
-    outer, inner = order[:2], order[2:]
-    far_arrive(outer)
-    far_experts(outer)
-    early = inner[:max(len(inner) - 2, 0)]
-    far_arrive(early)
-    far_return(outer[:1])
-    far_arrive(inner[len(early):])
-    far_return(outer[1:])
-    if inner:
-        far_experts(inner)
-        far_return(inner)
+    groups = [order[:2], order[2:-2], order[-2:]] if far > 4 else [order]
+    for i, js in enumerate(groups):
+        far_arrive(js)
+        far_experts(js)
+        far_return(js, 0)
+        if i < len(groups) - 2:
+            far_return(js, 1)
+    for js in groups[-2:]:
+        far_return(js, 1)
 
     own_w = hot(meta[...].astype(f32), me, True)
     near_w = [hot(mring[g, reach - 1].astype(f32), me, True) for g in range(2)]

time: 328 us -> 324 us (0.988)
  Pallas kernels: 327 us -> 323 us
    pallas_call x1, Pallas kernels: 327 us -> 323 us  [shards(): pl.pallas_call(functools.partial(kernel, n, reach, slots), out_shape=pltp...]
where the time goes in v6:
time: 324 us; the launch traced here: 323 us
  Pallas kernels  323 us (100%)
    pallas_call x1, Pallas kernels, shards(): pl.pallas_call(functools.partial(kernel, n, reach, slots), out_shape=pltp...  323 us

profile of v6, /device:TPU:37, one launch (start us, length us, event | category | flops | bytes accessed | tf_op | source)
XLA Modules:
  0.0 323.4 jit_solution(9897931724293709690)
XLA Ops:
  0.0 322.6 %shard_map.73 = bf16[128,2048]{1,0:T(8,128)(2,1)S(1)} custom-call(bf16[128,4096]{1,0:T(8,128)(2,1)} %tokens_hbm.1, f32[1,4096]{1,0:T(1,128)} %bitcast.3, s32[20,1,32]{2,1,0:T(1,128)} %bitcast.4, f32[20,1,32]{2,1,0:T(1,128)} %bitcast.5, bf16[1,4096,384]{2,1,0:T(8,128)(2,1)} %gate_hbm.1, bf16[1,4096,384]{2,1,0:T(8,128)(2,1)} %up_hbm.1, ...), custom_call_target="tpu_custom_call" | custom-call | tf_op jit(solution)/shard_map/pallas_call | solution.py:411
  322.6 0.8 copy.9

commit v7 on v6

--- a/solution.py
+++ b/solution.py
@@ -320,14 +320,18 @@
 
     order = list(range(far, 0, -1))
     groups = [order[:2], order[2:-2], order[-2:]] if far > 4 else [order]
+    held = []
     for i, js in enumerate(groups):
         far_arrive(js)
+        far_return(held[:1], 1)
         far_experts(js)
         far_return(js, 0)
+        far_return(held[1:], 1)
+        held = js
         if i < len(groups) - 2:
             far_return(js, 1)
-    for js in groups[-2:]:
-        far_return(js, 1)
+            held = []
+    far_return(held, 1)
 
     own_w = hot(meta[...].astype(f32), me, True)
     near_w = [hot(mring[g, reach - 1].astype(f32), me, True) for g in range(2)]

time: 324 us -> 325 us (level)
  no operation moved by 1% of the time
where the time goes in v7:
time: 325 us; the launch traced here: 324 us
  Pallas kernels  323 us (99%)
    pallas_call x1, Pallas kernels, shards(): pl.pallas_call(functools.partial(kernel, n, reach, slots), out_shape=pltp...  323 us

profile of v7, /device:TPU:37, one launch (start us, length us, event | category | flops | bytes accessed | tf_op | source)
XLA Modules:
  0.0 323.5 jit_solution(9310787655628931816)
XLA Ops:
  0.0 322.7 %shard_map.73 = bf16[128,2048]{1,0:T(8,128)(2,1)S(1)} custom-call(bf16[128,4096]{1,0:T(8,128)(2,1)} %tokens_hbm.1, f32[1,4096]{1,0:T(1,128)} %bitcast.3, s32[20,1,32]{2,1,0:T(1,128)} %bitcast.4, f32[20,1,32]{2,1,0:T(1,128)} %bitcast.5, bf16[1,4096,384]{2,1,0:T(8,128)(2,1)} %gate_hbm.1, bf16[1,4096,384]{2,1,0:T(8,128)(2,1)} %up_hbm.1, ...), custom_call_target="tpu_custom_call" | custom-call | tf_op jit(solution)/shard_map/pallas_call | solution.py:415
  322.7 0.8 copy.9

commit v8 on v6

--- a/solution.py
+++ b/solution.py
@@ -320,14 +320,34 @@
 
     order = list(range(far, 0, -1))
     groups = [order[:2], order[2:-2], order[-2:]] if far > 4 else [order]
-    for i, js in enumerate(groups):
-        far_arrive(js)
-        far_experts(js)
-        far_return(js, 0)
-        if i < len(groups) - 2:
-            far_return(js, 1)
-    for js in groups[-2:]:
-        far_return(js, 1)
+    last = groups[-1]
+
+    def far_left():
+        for j in last:
+            for g in range(2):
+                for p in parts_of(j):
+                    far_send(g, j, p).wait_send()
+
+    if len(groups) == 1:
+        far_arrive(last)
+        far_left()
+        far_experts(last)
+    else:
+        far_arrive(groups[0])
+        far_experts(groups[0])
+        far_arrive(groups[1])
+        far_left()
+        far_return(groups[0], 0)
+        far_return(groups[0], 1)
+        far_experts(groups[1])
+        far_return(groups[1], 0)
+        far_return(groups[1][:1], 1)
+        far_arrive(last)
+        far_experts(last)
+    far_return(last, 0)
+    if len(groups) > 1:
+        far_return(groups[1][1:], 1)
+    far_return(last, 1)
 
     own_w = hot(meta[...].astype(f32), me, True)
     near_w = [hot(mring[g, reach - 1].astype(f32), me, True) for g in range(2)]
@@ -391,7 +411,8 @@
         give(psf.at[j - 1], reach + j).wait_send()
         for g in range(2):
             for p in parts_of(j):
-                far_send(g, j, p).wait_send()
+                if j not in last:
+                    far_send(g, j, p).wait_send()
                 far_back(g, j, p).wait_send()
 
 

time: 324 us -> 324 us (level)
  no operation moved by 1% of the time
where the time goes in v8:
time: 324 us
  Pallas kernels  323 us (100%)
    pallas_call x1, Pallas kernels, shards(): pl.pallas_call(functools.partial(kernel, n, reach, slots), out_shape=pltp...  323 us

profile of v8, /device:TPU:37, one launch (start us, length us, event | category | flops | bytes accessed | tf_op | source)
XLA Modules:
  0.0 324.3 jit_solution(12516425579656360465)
XLA Ops:
  0.0 323.5 %shard_map.73 = bf16[128,2048]{1,0:T(8,128)(2,1)S(1)} custom-call(bf16[128,4096]{1,0:T(8,128)(2,1)} %tokens_hbm.1, f32[1,4096]{1,0:T(1,128)} %bitcast.3, s32[20,1,32]{2,1,0:T(1,128)} %bitcast.4, f32[20,1,32]{2,1,0:T(1,128)} %bitcast.5, bf16[1,4096,384]{2,1,0:T(8,128)(2,1)} %gate_hbm.1, bf16[1,4096,384]{2,1,0:T(8,128)(2,1)} %up_hbm.1, ...), custom_call_target="tpu_custom_call" | custom-call | tf_op jit(solution)/shard_map/pallas_call | solution.py:432
  323.5 0.8 copy.9
